TPU v7x, 512 devices: a whole 4x4x16 slice. The times are simulated.
512 devices in a mesh: sp: 128 (over z, x, core), tp: 4 (over y).
Axes of the slice: x: 4, y: 4, z: 16, core: 2. Of those that a mesh axis runs over, the one named last changes fastest.
Arguments:
- queries: bfloat16 [32768, 1024], P('sp', 'tp'), may hold values from -6 to 6
- keys: bfloat16 [32768, 1024], P('sp', 'tp'), may hold values from -6 to 6
- values: bfloat16 [32768, 2048], P('sp', 'tp'), may hold values from -6 to 6
- gate_code: bfloat16 [32768, 32], P('sp'), may hold values from -5.5 to 5.5
- gate_up: bfloat16 [32, 1024], P(None, 'tp'), may hold values from -1 to 1
- gate_bias: float32 [1024], P('tp'), as said below
- gla_gain: float32 [256], replicated, may hold values from 0.1 to 1.9
- conv_input: bfloat16 [32768, 2048], P('sp', 'tp'), may hold values from -6 to 6
- conv_gate: bfloat16 [32768, 2048], P('sp', 'tp'), may hold values from -6 to 6
- conv_taps: float32 [3, 2048], P(None, 'tp'), may hold values from -3.5 to 3.5
- out_gla: bfloat16 [2048, 2048], P('tp', 'sp'), may hold values from -0.09375 to 0.09375
- out_conv: bfloat16 [2048, 2048], P('tp', 'sp'), may hold values from -0.09375 to 0.09375
Outputs:
- mixed: bfloat16 [32768, 2048], P(('sp', 'tp'))
Inputs may be any that keep to these rules, and one draw needn't show every extreme that they name: `gate_bias`: every bias is at least 1.5, so every decay per step lies strictly between 0 and 1.
All inputs are finite; a program needn't handle non-finite values.
Results may differ from a plain program's by a relative error of at most 0.028.
Values may be sent and summed in bfloat16 or wider, within the bound.
A program may use at most 64 MiB of HBM per device.

v0:
```python
import jax
import jax.numpy as jnp
from jax import lax
from jax.sharding import Mesh
from jax.sharding import PartitionSpec as P

KEY_WIDTH = 128
HEAD_V = 256
SEGMENT_LENGTH = 64
SP = ("sp_0", "sp_1", "sp_2")
SP_TP = ("sp_0", "sp_1", "sp_2", "tp")
softness_divisor = 16.0
epsilon = 1.0


def split_up(x, dim, count):
    dims = x.shape
    parts = x.reshape(*dims[:dim], count, dims[dim] // count, *dims[dim + 1 :])
    return jnp.moveaxis(parts, dim, 0)


def laid_out(parts, dim):
    parts = jnp.moveaxis(parts, 0, dim)
    dims = parts.shape
    return parts.reshape(*dims[:dim], dims[dim] * dims[dim + 1], *dims[dim + 2 :])


def turned_blocks(parts, axes, turns):
    inside = parts.shape[1:]
    out = parts.reshape(*(lax.axis_size(a) for a in axes), *inside)
    for k in turns:
        out = lax.all_to_all(out, axes[k], k, k, tiled=True)
    return out.reshape(-1, *inside)


def exchange_by_chip(x, groups, turns, split_dim, concat_dim):
    count = lax.axis_size(groups[0]) * lax.axis_size(groups[1])
    parts = split_up(x, split_dim, count)
    return laid_out(turned_blocks(parts, groups, turns), concat_dim)


def all_blocks(x, axes, turns):
    parts = x[None]
    for k in turns:
        parts = lax.all_gather(parts, axes[k], axis=0, tiled=True)
    current = [lax.axis_size(axes[k]) for k in reversed(turns)]
    parts = parts.reshape(*current, *x.shape)
    turned = sorted(range(len(turns)), key=lambda place: turns[len(turns) - 1 - place])
    return parts.transpose(*turned, *range(len(turns), parts.ndim)).reshape(-1, *x.shape)


def whole_of(x, axes, turns, dim):
    return laid_out(all_blocks(x, axes, turns), dim)


def for_sending(x):
    return jax.tree.map(lambda a: a.astype(jnp.bfloat16) if a.dtype == jnp.float32 else a, x)


def from_behind(x, axis, by):
    count = lax.axis_size(axis)
    pairs = [(i, i + by) for i in range(count) if 0 <= i + by < count]
    return lax.ppermute(x, axis, pairs)


def turned_gather(arrays, axis, dims):
    turned = [jnp.moveaxis(a, dim, 0) for a, dim in zip(arrays, dims)]
    both = jnp.concatenate([t.reshape(len(t), -1) for t in turned], axis=1)
    out, at, outs = (lax.all_gather(both, axis, axis=0, tiled=True), 0, [])
    for t, dim in zip(turned, dims):
        piece = out[:, at : at + t[0].size].reshape(-1, *t.shape[1:])
        outs.append(jnp.moveaxis(piece, 0, dim))
        at += t[0].size
    return tuple(outs)


def sent_and_summed(x, axis, dim):
    parts = split_up(x, dim, lax.axis_size(axis))
    arrived = lax.all_to_all(parts, axis, split_axis=0, concat_axis=0, tiled=True)
    return arrived.astype(jnp.float32).sum(axis=0)


def chain(earlier, latter):
    return (earlier[0] * latter[0], latter[0][..., None] * earlier[1] + latter[1])


def per_device(
    queries,
    keys,
    values,
    gate_code,
    gate_up,
    gate_bias,
    gla_gain,
    conv_input,
    conv_gate,
    conv_taps,
    out_gla,
    out_conv,
):
    row_count = queries.shape[0]
    segment_count = row_count // SEGMENT_LENGTH
    head_count = queries.shape[1] // KEY_WIDTH
    gate_score = jnp.dot(gate_code, gate_up, preferred_element_type=jnp.float32) + gate_bias
    decay_logarithm = (jax.nn.log_sigmoid(gate_score) / softness_divisor).reshape(
        segment_count, SEGMENT_LENGTH, head_count, KEY_WIDTH
    )
    inside = jnp.cumsum(decay_logarithm, axis=1)
    seg_total = inside[:, -1]
    key_blocks = keys.reshape(segment_count, SEGMENT_LENGTH, head_count, KEY_WIDTH)
    scaled_keys = (key_blocks * jnp.exp(seg_total[:, None] - inside)).astype(jnp.bfloat16)
    value_blocks = values.reshape(segment_count, SEGMENT_LENGTH, head_count, HEAD_V)
    update = jnp.einsum(
        "nshk,nshv->nhkv", scaled_keys, value_blocks, preferred_element_type=jnp.float32
    )
    through, local_state = lax.associative_scan(chain, (jnp.exp(seg_total), update), axis=0)
    device_decay = through[-1]
    device_state = local_state[-1]
    columns = exchange_by_chip(
        device_state[None].astype(jnp.bfloat16), (("sp_0", "sp_1"), "sp_2"), (1, 0), 3, 0
    ).astype(jnp.float32)
    decays = whole_of(device_decay[None], SP, (0, 1, 2), 0)
    running = lax.associative_scan(chain, (decays, columns), axis=0)[1]
    before = jnp.concatenate([jnp.zeros_like(running[:1]), running[:-1]], axis=0)
    incoming = lax.all_to_all(
        for_sending(before), SP, split_axis=0, concat_axis=3, tiled=True
    ).astype(before.dtype)[0]
    states = local_state + through[..., None] * incoming[None]
    query_blocks = queries.reshape(segment_count, SEGMENT_LENGTH, head_count, KEY_WIDTH)
    readout = jnp.einsum(
        "nshk,nhkv->nshv",
        query_blocks,
        states.astype(jnp.bfloat16),
        preferred_element_type=jnp.float32,
    )
    norm_scale = lax.rsqrt(jnp.mean(readout * readout, axis=-1, keepdims=True) + epsilon)
    gla_mix = (
        (readout * norm_scale * gla_gain)
        .astype(jnp.bfloat16)
        .reshape(row_count, head_count * HEAD_V)
    )
    reach_rows = conv_taps.shape[0] - 1
    earlier_rows = from_behind(conv_input[row_count - reach_rows :], SP, 1)
    extended = jnp.concatenate([earlier_rows, conv_input], axis=0)
    convolved = jnp.zeros(conv_input.shape, jnp.float32)
    for offset in range(reach_rows + 1):
        convolved = convolved + conv_taps[offset] * extended[offset : offset + row_count]
    conv_mix = (conv_gate * convolved).astype(jnp.bfloat16)
    wide_gla, wide_conv = turned_gather((out_gla, out_conv), SP, (1, 1))
    summed = jnp.dot(gla_mix, wide_gla, preferred_element_type=jnp.float32)
    mixed_rows = sent_and_summed(
        (summed + jnp.dot(conv_mix, wide_conv, preferred_element_type=jnp.float32)).astype(
            jnp.bfloat16
        ),
        "tp",
        0,
    )
    return mixed_rows.astype(jnp.bfloat16)


def solution(mesh):
    split = Mesh(mesh.devices.reshape(16, 4, 2, mesh.shape["tp"]), ("sp_0", "sp_1", "sp_2", "tp"))
    placed = (
        P(SP, "tp"),
        P(SP, "tp"),
        P(SP, "tp"),
        P(SP, None),
        P(None, "tp"),
        P("tp"),
        P(),
        P(SP, "tp"),
        P(SP, "tp"),
        P(None, "tp"),
        P("tp", SP),
        P("tp", SP),
    )
    return jax.shard_map(
        per_device, mesh=split, in_specs=placed, out_specs=P(SP_TP, None), check_vma=False
    )
```

profile of v0, /device:TPU:1, one launch (start us, length us, event | category | flops | bytes accessed | tf_op | source)
XLA Modules:
  0.0 189.0 jit_solution(4269959149335231402)
XLA Ops:
  6.5 1.4 pad_maximum_fusion.6
  7.9 0.0 all-gather.5.cloned.1.call-update
  8.0 1.1 fusion.12
  9.0 0.1 reshape.75
  9.2 0.1 fusion.36
  9.4 0.1 reshape.83
  9.5 0.1 reshape.76
  9.6 0.2 multiply_convert_fusion.3
  9.8 0.3 fusion.14
  10.1 0.1 slice_add_fusion
  10.3 0.1 fusion.32
  10.4 0.1 fusion.31
  10.5 0.1 pad.73
  10.7 0.1 pad.74
  10.9 0.1 copy.69
  11.0 0.1 copy.70
  11.1 10.3 %all_to_all.24 = bf16[64,2,1,2,128,2]{4,5,0,3,2,1:T(2,128)(2,1)S(1)} all-to-all(bf16[64,2,1,2,128,2]{4,5,0,3,2,1:T(2,128)(2,1)S(1)} %copy.70), channel_id=1, replica_groups=mesh['sp_0'=16,'sp_1'=4,'sp_2'=2,'tp'=4] {'sp_2'}, dimensions={1} | all-to-all | bytes 262144 | tf_op jit(solution)/shard_map/all_to_all | solution.py:32
  21.4 0.7 copy.71
  22.2 12.9 %all-to-all-start.1 = ((bf16[64,2,1,2,128,2]{4,5,1,3,2,0:T(2,128)(2,1)}), bf16[64,2,1,2,128,2]{4,5,1,3,2,0:T(2,128)(2,1)S(1)}, u32[]{:S(2)}, u32[]{:S(2)}) async-start(bf16[64,2,1,2,128,2]{4,5,1,3,2,0:T(2,128)(2,1)} %copy.71), calls=%async_computation.1 | async-start | bytes 262144 | tf_op jit(solution)/shard_map/all_to_all | solution.py:32
  35.2 25.6 %all-gather = f32[16,2,128]{2,1,0:T(2,128)S(1)} all-gather(f32[1,2,128]{2,1,0:T(2,128)S(1)} %slice_add_fusion.4), channel_id=2, replica_groups=mesh['sp_0'=16,'sp_1'=4,'sp_2'=2,'tp'=4] {'sp_0'}, dimensions={0}, use_global_device_ids=true | all-gather | bytes 17408 | tf_op jit(solution)/shard_map/all_gather | solution.py:45
  60.8 10.3 %all-gather.1 = f32[64,2,128]{2,1,0:T(2,128)S(1)} all-gather(f32[16,2,128]{2,1,0:T(2,128)S(1)} %all-gather), channel_id=3, replica_groups=mesh['sp_0'=16,'sp_1'=4,'sp_2'=2,'tp'=4] {'sp_1'}, dimensions={0}, use_global_device_ids=true | all-gather | bytes 81920 | tf_op jit(solution)/shard_map/all_gather | solution.py:45
  71.1 9.7 %all-gather.2 = f32[128,2,128]{2,1,0:T(2,128)S(1)} all-gather(f32[64,2,128]{2,1,0:T(2,128)S(1)} %all-gather.1), channel_id=4, replica_groups=mesh['sp_0'=16,'sp_1'=4,'sp_2'=2,'tp'=4] {'sp_2'}, dimensions={0}, use_global_device_ids=true | all-gather | bytes 196608 | tf_op jit(solution)/shard_map/all_gather | solution.py:45
  80.8 0.1 copy.74
  81.4 0.2 copy.73
  81.6 0.1 slice.267
  81.7 0.1 slice.268
  81.8 0.1 slice.273
  81.9 0.1 slice.274
  82.0 0.1 slice.279
  82.0 0.1 slice.280
  82.1 0.1 slice.285
  82.2 0.1 slice.286
  82.3 0.1 slice.291
  82.4 0.1 slice.292
  82.5 0.1 slice.297
  82.6 0.1 slice.298
  82.6 0.1 slice.306
  82.7 0.1 slice.308
  82.8 0.1 slice.310
  82.9 0.1 slice.312
  83.0 0.1 slice.314
  83.2 0.1 pad.81
  83.3 0.1 pad.82
  83.8 0.0 copy-start.7
  84.0 0.1 pad.190
  84.1 0.1 pad.116
  84.2 0.1 copy.80
  84.3 0.8 concatenate.41.clone
  85.1 13.7 %all-to-all-start.2 = ((bf16[128,2,128,2]{2,3,1,0:T(2,128)(2,1)}), bf16[128,2,128,2]{2,3,1,0:T(2,128)(2,1)S(1)}, u32[]{:S(2)}, u32[]{:S(2)}) async-start(bf16[128,2,128,2]{2,3,1,0:T(2,128)(2,1)} %concatenate.41.clone), calls=%async_computation.2 | async-start | bytes 262144 | tf_op jit(solution)/shard_map/all_to_all | solution.py:125
  98.8 3.5 %collective-permute-start = (bf16[2,512]{1,0:T(2,128)(2,1)S(1)}, bf16[2,512]{1,0:T(2,128)(2,1)S(1)}, u32[]{:S(2)}, u32[]{:S(2)}) collective-permute-start(bf16[2,512]{1,0:T(2,128)(2,1)S(1)} %slice.318), channel_id=1, source_target_pairs={{0,4},{4,8},{8,12},{12,16},{16,20},{20,24},{24,28},{28,32},{32,36}... | collective-permute-start | bytes 6152 | tf_op jit(solution)/shard_map/ppermute | solution.py:63
  102.5 12.7 %all-to-all-done.2 = bf16[128,2,128,2]{2,3,1,0:T(2,128)(2,1)S(1)} async-done(((bf16[128,2,128,2]{2,3,1,0:T(2,128)(2,1)}), bf16[128,2,128,2]{2,3,1,0:T(2,128)(2,1)S(1)}, u32[]{:S(2)}, u32[]{:S(2)}) %all-to-all-start.2) | async-done | bytes 131104 | tf_op jit(solution)/shard_map/all_to_all | solution.py:125
  115.1 0.1 convert_bitcast_fusion
  115.2 0.1 copy.76
  115.3 0.1 copy.77
  115.5 0.5 multiply_reduce_fusion
  115.9 0.1 multiply_convert_fusion.1
  116.1 0.3 copy.79
  116.4 42.7 %all-gather.5.cloned.1.call-done = bf16[2048,1024]{1,0:T(8,128)(2,1)} async-done(((bf16[16,1024]{1,0:T(8,128)(2,1)}), bf16[2048,1024]{1,0:T(8,128)(2,1)}) %all-gather.5.cloned.1.call-update) | async-done | bytes 4194320 | tf_op jit(solution)/shard_map/all_gather | solution.py:69
  159.1 2.5 %fusion.2 = f32[256,2048]{1,0:T(8,128)S(1)} fusion(bf16[256,512]{1,0:T(8,128)(2,1)S(1)} %bitcast.45, bf16[2048,1024]{1,0:T(8,128)(2,1)} %all-gather.5.cloned.1.call-done), kind=kOutput, calls=%fused_computation.3 | convolution fusion | flops 536870912 | bytes 4456448 | tf_op jit(solution)/shard_map/dot_general | solution.py:150
  161.6 0.3 copy-done.1
  161.9 0.0 copy-done.8
  162.0 0.9 fusion
  162.8 18.4 %all_to_all.25 = bf16[4,64,2048]{2,1,0:T(8,128)(2,1)S(1)} all-to-all(bf16[4,64,2048]{2,1,0:T(8,128)(2,1)S(1)} %bitcast.46), channel_id=1, replica_groups=mesh['sp_0'=16,'sp_1'=4,'sp_2'=2,'tp'=4] {'tp'}, dimensions={0} | all-to-all | bytes 2097152 | tf_op jit(solution)/shard_map/all_to_all | solution.py:79
  181.3 0.9 reduce_sum.22
  (101 shorter events, 1.3 us)
Async XLA Ops:
  6.5 1.4 copy-start
  6.5 2.8 %copy-start.3 = (bf16[256,256]{1,0:T(8,128)(2,1)S(1)}, bf16[256,256]{1,0:T(8,128)(2,1)}, u32[]{:S(2)}) copy-start(bf16[256,256]{1,0:T(8,128)(2,1)} %param.13) | copy-start | bytes 393220
  6.5 3.0 %copy-start.2 = (bf16[256,512]{1,0:T(8,128)(2,1)S(1)}, bf16[256,512]{1,0:T(8,128)(2,1)}, u32[]{:S(2)}) copy-start(bf16[256,512]{1,0:T(8,128)(2,1)} %param.14) | copy-start | bytes 786436
  6.5 152.6 %all-gather.5.cloned.1.call-start = ((), (), s32[]{:S(2)}) async-start(), calls=%async_computation.4 | async-start | bytes 4227072 | tf_op jit(solution)/shard_map/all_gather | solution.py:69
  22.2 59.1 %all-to-all-start.1 = ((bf16[64,2,1,2,128,2]{4,5,1,3,2,0:T(2,128)(2,1)}), bf16[64,2,1,2,128,2]{4,5,1,3,2,0:T(2,128)(2,1)S(1)}, u32[]{:S(2)}, u32[]{:S(2)}) async-start(bf16[64,2,1,2,128,2]{4,5,1,3,2,0:T(2,128)(2,1)} %copy.71), calls=%async_computation.1 | async-start | bytes 262144 | tf_op jit(solution)/shard_map/all_to_all | solution.py:32
  83.8 15.0 %copy-start.7 = (bf16[256,512]{1,0:T(8,128)(2,1)S(1)}, bf16[256,512]{1,0:T(8,128)(2,1)}, u32[]{:S(2)}) copy-start(bf16[256,512]{1,0:T(8,128)(2,1)} %param.19) | copy-start | bytes 786436
  83.8 18.6 %copy-start.4 = (bf16[256,256]{1,0:T(8,128)(2,1)S(1)}, bf16[256,256]{1,0:T(8,128)(2,1)}, u32[]{:S(2)}) copy-start(bf16[256,256]{1,0:T(8,128)(2,1)} %param.12) | copy-start | bytes 393220
  83.8 18.6 %copy-start.5 = (f32[3,512]{1,0:T(4,128)S(1)}, f32[3,512]{1,0:T(4,128)}, u32[]{:S(2)}) copy-start(f32[3,512]{1,0:T(4,128)} %param.21) | copy-start | bytes 18436
  85.1 30.0 %all-to-all-start.2 = ((bf16[128,2,128,2]{2,3,1,0:T(2,128)(2,1)}), bf16[128,2,128,2]{2,3,1,0:T(2,128)(2,1)S(1)}, u32[]{:S(2)}, u32[]{:S(2)}) async-start(bf16[128,2,128,2]{2,3,1,0:T(2,128)(2,1)} %concatenate.41.clone), calls=%async_computation.2 | async-start | bytes 262144 | tf_op jit(solution)/shard_map/all_to_all | solution.py:125
  98.8 62.8 %collective-permute-start = (bf16[2,512]{1,0:T(2,128)(2,1)S(1)}, bf16[2,512]{1,0:T(2,128)(2,1)S(1)}, u32[]{:S(2)}, u32[]{:S(2)}) collective-permute-start(bf16[2,512]{1,0:T(2,128)(2,1)S(1)} %slice.318), channel_id=1, source_target_pairs={{0,4},{4,8},{8,12},{12,16},{16,20},{20,24},{24,28},{28,32},{32,36}... | collective-permute-start | bytes 6152 | tf_op jit(solution)/shard_map/ppermute | solution.py:63
  115.2 0.7 copy-start.6
  159.1 2.8 %copy-start.1 = (bf16[2048,1024]{1,0:T(8,128)(2,1)S(1)}, bf16[2048,1024]{1,0:T(8,128)(2,1)}, u32[]{:S(2)}) copy-start(bf16[2048,1024]{1,0:T(8,128)(2,1)} %all-gather.5.cloned.1.call-done) | copy-start | bytes 12582916
  159.1 2.8 %copy-start.8 = (bf16[256,512]{1,0:T(8,128)(2,1)S(1)}, bf16[256,512]{1,0:T(8,128)(2,1)}, u32[]{:S(2)}) copy-start(bf16[256,512]{1,0:T(8,128)(2,1)} %param.20) | copy-start | bytes 786436
Sparse Core Ops, SparseCore 0:
  10.5 148.5 all-gather.4
where the time goes:
time: 189 us
  blocking collectives  74.3 us (39%)
  waiting for transfers between devices  55.4 us (29%)
  starting transfers between devices  30.2 us (16%)
  between operations  14.3 us (8%)
  local copies, waits for them, and re-layouts  5.91 us (3%)
  matrix products  5.23 us (3%)
  other arithmetic  3.7 us (2%)
    all_gather x3, blocking collectives, all_blocks(): parts = lax.all_gather(parts, axes[k], axis=0, tiled=True)  45.6 us
    all_gather x1, waiting for transfers between devices, turned_gather(): out, at, outs = (lax.all_gather(both, axis, axis=0, tiled=True), 0, [])  42.7 us
    all_to_all x1, blocking collectives, sent_and_summed(): lax.all_to_all(parts, axis, split_axis=0, concat_axis=0, tiled=True)  18.4 us
    all_to_all x1, starting transfers between devices, per_device(): lax.all_to_all(for_sending(before), SP, split_axis=0, concat_axis=3, tile...  13.7 us
    all_to_all x1, starting transfers between devices, turned_blocks(): out = lax.all_to_all(out, axes[k], k, k, tiled=True)  12.9 us
    all_to_all x1, waiting for transfers between devices, per_device(): lax.all_to_all(for_sending(before), SP, split_axis=0, concat_axis=3, tile...  12.7 us
    all_to_all x1, blocking collectives, turned_blocks(): out = lax.all_to_all(out, axes[k], k, k, tiled=True)  10.3 us
  transfers between devices with their start and end apart: 4, of which 2 were waited for; matrix products, arithmetic and copies ran while one was open for 6% of the time, Pallas kernels for 0%

commit v1 on v0

--- a/solution.py
+++ b/solution.py
@@ -42,7 +42,9 @@
 def all_blocks(x, axes, turns):
     parts = x[None]
     for k in turns:
-        parts = lax.all_gather(parts, axes[k], axis=0, tiled=True)
+        parts = jnp.concatenate(
+            lax.all_to_all(jnp.stack([parts] * lax.axis_size(axes[k])), axes[k], 0, 0), axis=0
+        )
     current = [lax.axis_size(axes[k]) for k in reversed(turns)]
     parts = parts.reshape(*current, *x.shape)
     turned = sorted(range(len(turns)), key=lambda place: turns[len(turns) - 1 - place])

time: 189 us -> 204 us (1.079)
  waiting for transfers between devices: 55.4 us -> 106 us
  blocking collectives: 74.3 us -> 23.7 us
  starting transfers between devices: 30.2 us -> 41.8 us
  local copies, waits for them, and re-layouts: 5.91 us -> 8.51 us
    all_gather x3 -> x0, blocking collectives: 45.6 us -> none  [all_blocks(): parts = lax.all_gather(parts, axes[k], axis=0, tiled=True)]
    all_gather x1, waiting for transfers between devices: 42.7 us -> 66.1 us  [turned_gather(): out, at, outs = (lax.all_gather(both, axis, axis=0, tiled=True), 0, [])]
    all_to_all x0 -> x2, starting transfers between devices: none -> 19.7 us  [all_blocks(): lax.all_to_all(jnp.stack([parts] * lax.axis_size(axes[k])), axes[k], 0, 0)]
    all_to_all x1 -> x2, waiting for transfers between devices: 0.01 us -> 16.2 us  [turned_blocks(): out = lax.all_to_all(out, axes[k], k, k, tiled=True)]
    all_to_all x0 -> x2, waiting for transfers between devices: none -> 11.3 us  [all_blocks(): lax.all_to_all(jnp.stack([parts] * lax.axis_size(axes[k])), axes[k], 0, 0)]
    all_to_all x1, starting transfers between devices: 13.7 us -> 8.45 us  [per_device(): lax.all_to_all(for_sending(before), SP, split_axis=0, concat_axis=3, tile...]
    all_to_all x1, blocking collectives: 10.3 us -> 5.27 us  [all_blocks(): lax.all_to_all(jnp.stack([parts] * lax.axis_size(axes[k])), axes[k], 0, 0)]
    all_to_all x1 -> x2, starting transfers between devices: 12.9 us -> 10.1 us  [turned_blocks(): out = lax.all_to_all(out, axes[k], k, k, tiled=True)]
  transfers between devices with their start and end apart: 4 -> 7, of which waited for: 2 -> 6; matrix products, arithmetic and copies ran while one was open for 6% -> 6% of each run, Pallas kernels for 0% -> 0%
where the time goes in v1:
time: 204 us
  waiting for transfers between devices  106 us (52%)
  starting transfers between devices  41.8 us (20%)
  blocking collectives  23.7 us (12%)
  between operations  14.3 us (7%)
  local copies, waits for them, and re-layouts  8.51 us (4%)
  matrix products  5.22 us (3%)
  other arithmetic  3.66 us (2%)
    all_gather x1, waiting for transfers between devices, turned_gather(): out, at, outs = (lax.all_gather(both, axis, axis=0, tiled=True), 0, [])  66.1 us
    all_to_all x2, starting transfers between devices, all_blocks(): lax.all_to_all(jnp.stack([parts] * lax.axis_size(axes[k])), axes[k], 0, 0)  19.7 us
    all_to_all x1, blocking collectives, sent_and_summed(): lax.all_to_all(parts, axis, split_axis=0, concat_axis=0, tiled=True)  18.4 us
    all_to_all x2, waiting for transfers between devices, turned_blocks(): out = lax.all_to_all(out, axes[k], k, k, tiled=True)  16.2 us
    all_to_all x1, waiting for transfers between devices, per_device(): lax.all_to_all(for_sending(before), SP, split_axis=0, concat_axis=3, tile...  12.6 us
    all_to_all x2, waiting for transfers between devices, all_blocks(): lax.all_to_all(jnp.stack([parts] * lax.axis_size(axes[k])), axes[k], 0, 0)  11.3 us
    all_to_all x2, starting transfers between devices, turned_blocks(): out = lax.all_to_all(out, axes[k], k, k, tiled=True)  10.1 us
    all_to_all x1, starting transfers between devices, per_device(): lax.all_to_all(for_sending(before), SP, split_axis=0, concat_axis=3, tile...  8.45 us
  transfers between devices with their start and end apart: 7, of which 6 were waited for; matrix products, arithmetic and copies ran while one was open for 6% of the time, Pallas kernels for 0%

profile of v1, /device:TPU:1, one launch (start us, length us, event | category | flops | bytes accessed | tf_op | source)
XLA Modules:
  0.0 203.5 jit_solution(1644748539338391772)
XLA Ops:
  6.5 0.7 copy-done
  7.3 1.1 fusion.12
  8.3 0.1 reshape.79
  8.5 0.1 fusion.36
  8.7 0.6 stack.9
  9.3 15.7 %all-to-all-start.2 = ((f32[16,1,1,2,128]{4,3,2,1,0:T(2,128)}), f32[16,1,1,2,128]{4,3,2,1,0:T(2,128)S(1)}, u32[]{:S(2)}, u32[]{:S(2)}) async-start(f32[16,1,1,2,128]{4,3,2,1,0:T(2,128)} %stack.9), calls=%async_computation.2 | async-start | bytes 32768 | tf_op jit(solution)/shard_map/all_to_all | solution.py:46
  25.1 1.3 pad_maximum_fusion.7
  26.5 0.1 reshape.86
  26.6 0.1 reshape.80
  26.7 0.2 multiply_convert_fusion.3
  26.9 0.3 fusion.14
  27.3 0.1 slice_add_fusion
  27.4 0.1 fusion.32
  27.5 0.1 fusion.31
  27.7 0.1 pad.73
  27.8 0.1 pad.74
  28.0 0.1 copy.89
  28.1 0.8 copy.90
  28.9 7.6 %all-to-all-done.2 = f32[16,1,1,2,128]{4,3,2,1,0:T(2,128)S(1)} async-done(((f32[16,1,1,2,128]{4,3,2,1,0:T(2,128)}), f32[16,1,1,2,128]{4,3,2,1,0:T(2,128)S(1)}, u32[]{:S(2)}, u32[]{:S(2)}) %all-to-all-start.2) | async-done | bytes 16416 | tf_op jit(solution)/shard_map/all_to_all | solution.py:46
  36.5 5.4 %all-to-all-start = ((bf16[64,2,1,2,128,2]{4,5,0,3,2,1:T(2,128)(2,1)}), bf16[64,2,1,2,128,2]{4,5,0,3,2,1:T(2,128)(2,1)S(1)}, u32[]{:S(2)}, u32[]{:S(2)}) async-start(bf16[64,2,1,2,128,2]{4,5,0,3,2,1:T(2,128)(2,1)} %copy.90), calls=%async_computation | async-start | bytes 262144 | tf_op jit(solution)/shard_map/all_to_all | solution.py:32
  41.9 1.1 all-to-all-done
  43.0 0.6 stack.10
  43.6 4.0 %all-to-all-start.3 = ((f32[4,16,1,2,128]{4,1,3,2,0:T(8,128)}), f32[4,16,1,2,128]{4,1,3,2,0:T(8,128)S(1)}, u32[]{:S(2)}, u32[]{:S(2)}) async-start(f32[4,16,1,2,128]{4,1,3,2,0:T(8,128)} %stack.10), calls=%async_computation.3 | async-start | bytes 131072 | tf_op jit(solution)/shard_map/all_to_all | solution.py:46
  47.6 0.7 copy.91
  48.4 3.7 %all-to-all-done.3 = f32[4,16,1,2,128]{4,1,3,2,0:T(8,128)S(1)} async-done(((f32[4,16,1,2,128]{4,1,3,2,0:T(8,128)}), f32[4,16,1,2,128]{4,1,3,2,0:T(8,128)S(1)}, u32[]{:S(2)}, u32[]{:S(2)}) %all-to-all-start.3) | async-done | bytes 65568 | tf_op jit(solution)/shard_map/all_to_all | solution.py:46
  52.1 5.3 %all_to_all.39 = f32[2,64,1,2,128]{4,1,3,2,0:T(8,128)S(1)} all-to-all(f32[2,64,1,2,128]{4,1,3,2,0:T(8,128)S(1)} %pad_maximum_fusion.3), channel_id=1, replica_groups=mesh['sp_0'=16,'sp_1'=4,'sp_2'=2,'tp'=4] {'sp_2'}, dimensions={0} | all-to-all | bytes 262144 | tf_op jit(solution)/shard_map/all_to_all | solution.py:46
  57.4 4.6 %all-to-all-start.1 = ((bf16[64,2,1,2,128,2]{4,5,1,3,2,0:T(2,128)(2,1)}), bf16[64,2,1,2,128,2]{4,5,1,3,2,0:T(2,128)(2,1)S(1)}, u32[]{:S(2)}, u32[]{:S(2)}) async-start(bf16[64,2,1,2,128,2]{4,5,1,3,2,0:T(2,128)(2,1)} %copy.91), calls=%async_computation.1 | async-start | bytes 262144 | tf_op jit(solution)/shard_map/all_to_all | solution.py:32
  62.0 0.1 copy.96
  62.6 15.1 %all-to-all-done.1 = bf16[64,2,1,2,128,2]{4,5,1,3,2,0:T(2,128)(2,1)S(1)} async-done(((bf16[64,2,1,2,128,2]{4,5,1,3,2,0:T(2,128)(2,1)}), bf16[64,2,1,2,128,2]{4,5,1,3,2,0:T(2,128)(2,1)S(1)}, u32[]{:S(2)}, u32[]{:S(2)}) %all-to-all-start.1) | async-done | bytes 131104 | tf_op jit(solution)/shard_map/all_to_all | solution.py:32
  77.7 0.2 copy.93
  77.9 0.1 slice.270
  78.0 0.1 slice.271
  78.1 0.1 slice.276
  78.2 0.1 slice.277
  78.3 0.1 slice.282
  78.4 0.1 slice.283
  78.5 0.1 slice.288
  78.6 0.1 slice.289
  78.7 0.1 slice.294
  78.7 0.1 slice.295
  78.8 0.1 slice.300
  78.9 0.1 slice.301
  79.0 0.1 slice.309
  79.1 0.1 slice.311
  79.2 0.1 slice.313
  79.3 0.1 slice.315
  79.4 0.1 slice.317
  80.6 0.1 copy.102
  80.7 0.8 concatenate.41.clone
  81.5 8.5 %all-to-all-start.5 = ((bf16[128,2,128,2]{2,3,1,0:T(2,128)(2,1)}), bf16[128,2,128,2]{2,3,1,0:T(2,128)(2,1)S(1)}, u32[]{:S(2)}, u32[]{:S(2)}) async-start(bf16[128,2,128,2]{2,3,1,0:T(2,128)(2,1)} %concatenate.41.clone), calls=%async_computation.5 | async-start | bytes 262144 | tf_op jit(solution)/shard_map/all_to_all | solution.py:127
  89.9 3.5 %collective-permute-start = (bf16[2,512]{1,0:T(2,128)(2,1)S(1)}, bf16[2,512]{1,0:T(2,128)(2,1)S(1)}, u32[]{:S(2)}, u32[]{:S(2)}) collective-permute-start(bf16[2,512]{1,0:T(2,128)(2,1)S(1)} %slice.321), channel_id=1, source_target_pairs={{0,4},{4,8},{8,12},{12,16},{16,20},{20,24},{24,28},{28,32},{32,36}... | collective-permute-start | bytes 6152 | tf_op jit(solution)/shard_map/ppermute | solution.py:65
  93.6 12.6 %all-to-all-done.5 = bf16[128,2,128,2]{2,3,1,0:T(2,128)(2,1)S(1)} async-done(((bf16[128,2,128,2]{2,3,1,0:T(2,128)(2,1)}), bf16[128,2,128,2]{2,3,1,0:T(2,128)(2,1)S(1)}, u32[]{:S(2)}, u32[]{:S(2)}) %all-to-all-start.5) | async-done | bytes 131104 | tf_op jit(solution)/shard_map/all_to_all | solution.py:127
  106.2 0.1 convert_bitcast_fusion
  106.3 0.1 copy.98
  106.4 0.1 copy.99
  106.5 0.5 multiply_reduce_fusion
  107.0 0.1 multiply_convert_fusion.1
  107.2 0.3 copy.101
  107.5 66.1 %all-gather.2.cloned.1.call-done = bf16[2048,1024]{1,0:T(8,128)(2,1)} async-done(((bf16[16,1024]{1,0:T(8,128)(2,1)}), bf16[2048,1024]{1,0:T(8,128)(2,1)}) %all-gather.2.cloned.1.call-update) | async-done | bytes 4194320 | tf_op jit(solution)/shard_map/all_gather | solution.py:71
  173.6 2.5 %fusion.2 = f32[256,2048]{1,0:T(8,128)S(1)} fusion(bf16[256,512]{1,0:T(8,128)(2,1)S(1)} %bitcast.49, bf16[2048,1024]{1,0:T(8,128)(2,1)} %all-gather.2.cloned.1.call-done), kind=kOutput, calls=%fused_computation.3 | convolution fusion | flops 536870912 | bytes 4456448 | tf_op jit(solution)/shard_map/dot_general | solution.py:152
  176.1 0.3 copy-done.1
  176.4 0.9 fusion
  177.3 18.4 %all_to_all.40 = bf16[4,64,2048]{2,1,0:T(8,128)(2,1)S(1)} all-to-all(bf16[4,64,2048]{2,1,0:T(8,128)(2,1)S(1)} %bitcast.50), channel_id=1, replica_groups=mesh['sp_0'=16,'sp_1'=4,'sp_2'=2,'tp'=4] {'tp'}, dimensions={0} | all-to-all | bytes 2097152 | tf_op jit(solution)/shard_map/all_to_all | solution.py:81
  195.7 0.9 reduce_sum.22
  (109 shorter events, 1.7 us)
Async XLA Ops:
  6.5 0.7 copy-start
  6.5 19.9 %copy-start.3 = (bf16[256,256]{1,0:T(8,128)(2,1)S(1)}, bf16[256,256]{1,0:T(8,128)(2,1)}, u32[]{:S(2)}) copy-start(bf16[256,256]{1,0:T(8,128)(2,1)} %param.13) | copy-start | bytes 393220
  6.5 20.1 %copy-start.2 = (bf16[256,512]{1,0:T(8,128)(2,1)S(1)}, bf16[256,512]{1,0:T(8,128)(2,1)}, u32[]{:S(2)}) copy-start(bf16[256,512]{1,0:T(8,128)(2,1)} %param.14) | copy-start | bytes 786436
  9.3 27.1 %all-to-all-start.2 = ((f32[16,1,1,2,128]{4,3,2,1,0:T(2,128)}), f32[16,1,1,2,128]{4,3,2,1,0:T(2,128)S(1)}, u32[]{:S(2)}, u32[]{:S(2)}) async-start(f32[16,1,1,2,128]{4,3,2,1,0:T(2,128)} %stack.9), calls=%async_computation.2 | async-start | bytes 32768 | tf_op jit(solution)/shard_map/all_to_all | solution.py:46
  25.1 148.5 %all-gather.2.cloned.1.call-start = ((), (), s32[]{:S(2)}) async-start(), calls=%async_computation.7 | async-start | bytes 4227072 | tf_op jit(solution)/shard_map/all_gather | solution.py:71
  36.5 6.6 %all-to-all-start = ((bf16[64,2,1,2,128,2]{4,5,0,3,2,1:T(2,128)(2,1)}), bf16[64,2,1,2,128,2]{4,5,0,3,2,1:T(2,128)(2,1)S(1)}, u32[]{:S(2)}, u32[]{:S(2)}) async-start(bf16[64,2,1,2,128,2]{4,5,0,3,2,1:T(2,128)(2,1)} %copy.90), calls=%async_computation | async-start | bytes 262144 | tf_op jit(solution)/shard_map/all_to_all | solution.py:32
  43.6 8.5 %all-to-all-start.3 = ((f32[4,16,1,2,128]{4,1,3,2,0:T(8,128)}), f32[4,16,1,2,128]{4,1,3,2,0:T(8,128)S(1)}, u32[]{:S(2)}, u32[]{:S(2)}) async-start(f32[4,16,1,2,128]{4,1,3,2,0:T(8,128)} %stack.10), calls=%async_computation.3 | async-start | bytes 131072 | tf_op jit(solution)/shard_map/all_to_all | solution.py:46
  57.4 20.3 %all-to-all-start.1 = ((bf16[64,2,1,2,128,2]{4,5,1,3,2,0:T(2,128)(2,1)}), bf16[64,2,1,2,128,2]{4,5,1,3,2,0:T(2,128)(2,1)S(1)}, u32[]{:S(2)}, u32[]{:S(2)}) async-start(bf16[64,2,1,2,128,2]{4,5,1,3,2,0:T(2,128)(2,1)} %copy.91), calls=%async_computation.1 | async-start | bytes 262144 | tf_op jit(solution)/shard_map/all_to_all | solution.py:32
  80.1 9.8 %copy-start.7 = (bf16[256,512]{1,0:T(8,128)(2,1)S(1)}, bf16[256,512]{1,0:T(8,128)(2,1)}, u32[]{:S(2)}) copy-start(bf16[256,512]{1,0:T(8,128)(2,1)} %param.19) | copy-start | bytes 786436
  80.1 13.4 %copy-start.4 = (bf16[256,256]{1,0:T(8,128)(2,1)S(1)}, bf16[256,256]{1,0:T(8,128)(2,1)}, u32[]{:S(2)}) copy-start(bf16[256,256]{1,0:T(8,128)(2,1)} %param.12) | copy-start | bytes 393220
  80.2 13.4 %copy-start.5 = (f32[3,512]{1,0:T(4,128)S(1)}, f32[3,512]{1,0:T(4,128)}, u32[]{:S(2)}) copy-start(f32[3,512]{1,0:T(4,128)} %param.21) | copy-start | bytes 18436
  81.5 24.7 %all-to-all-start.5 = ((bf16[128,2,128,2]{2,3,1,0:T(2,128)(2,1)}), bf16[128,2,128,2]{2,3,1,0:T(2,128)(2,1)S(1)}, u32[]{:S(2)}, u32[]{:S(2)}) async-start(bf16[128,2,128,2]{2,3,1,0:T(2,128)(2,1)} %concatenate.41.clone), calls=%async_computation.5 | async-start | bytes 262144 | tf_op jit(solution)/shard_map/all_to_all | solution.py:127
  89.9 86.1 %collective-permute-start = (bf16[2,512]{1,0:T(2,128)(2,1)S(1)}, bf16[2,512]{1,0:T(2,128)(2,1)S(1)}, u32[]{:S(2)}, u32[]{:S(2)}) collective-permute-start(bf16[2,512]{1,0:T(2,128)(2,1)S(1)} %slice.321), channel_id=1, source_target_pairs={{0,4},{4,8},{8,12},{12,16},{16,20},{20,24},{24,28},{28,32},{32,36}... | collective-permute-start | bytes 6152 | tf_op jit(solution)/shard_map/ppermute | solution.py:65
  106.3 0.7 copy-start.6
  173.6 2.8 %copy-start.1 = (bf16[2048,1024]{1,0:T(8,128)(2,1)S(1)}, bf16[2048,1024]{1,0:T(8,128)(2,1)}, u32[]{:S(2)}) copy-start(bf16[2048,1024]{1,0:T(8,128)(2,1)} %all-gather.2.cloned.1.call-done) | copy-start | bytes 12582916
  173.6 2.8 %copy-start.8 = (bf16[256,512]{1,0:T(8,128)(2,1)S(1)}, bf16[256,512]{1,0:T(8,128)(2,1)}, u32[]{:S(2)}) copy-start(bf16[256,512]{1,0:T(8,128)(2,1)} %param.20) | copy-start | bytes 786436
Sparse Core Ops, SparseCore 0:
  29.0 144.5 all-gather.1
